TPU v7x, 32 devices: a whole 2x2x4 slice. The times are simulated.
32 devices in a mesh: fs: 8 (over z, y), tp: 4 (over x, core).
Axes of the slice: x: 2, y: 2, z: 4, core: 2. Of those that a mesh axis runs over, the one named last changes fastest.
Arguments:
- tokens: bfloat16 [8192, 2048], P('fs'), may hold values from -6 to 6
- norm_gain: float32 [2048], P('fs'), may hold values from 0.1 to 1.9
- gate_train: float32 [8, 2048, 768], P(None, 'fs', 'tp'), may hold values from -0.125 to 0.125
- up_train: float32 [8, 2048, 768], P(None, 'fs', 'tp'), may hold values from -0.125 to 0.125
- down_train: float32 [8, 768, 2048], P(None, 'fs', 'tp'), may hold values from -0.21875 to 0.21875
- expert_ids: int32 [8192, 2], P('fs'), may hold values from 0 to 7, all different within a row; in each aligned block of 1024 rows (0 to 1023, 1024 to 2047, ...) at most 512 rows name the same one
- route_weights: float32 [8192, 2], P('fs'), may hold values from 0.1 to 1
Outputs:
- gate_serve: bfloat16 [8, 2048, 768], P('fs', None, 'tp')
- up_serve: bfloat16 [8, 2048, 768], P('fs', None, 'tp')
- down_serve: bfloat16 [8, 768, 2048], P('fs', 'tp')
- mixed: bfloat16 [8192, 2048], P('fs', 'tp')
Inputs may be any that keep to these rules, and one draw needn't show every extreme that they name: `expert_ids`: each row names 2 different experts. Within each aligned block of 1024 rows no expert is named more than 512 times, and in every block some expert is named exactly 512 times; every expert is named somewhere.
All inputs are finite; a program needn't handle non-finite values.
Results may differ from a plain program's by a relative error of at most 0.011.
Values may be sent and summed in bfloat16 or wider, within the bound.
A program may use at most 128 MiB of HBM per device.

v0:
```python
import jax
import jax.numpy as jnp
from jax import lax
from jax.sharding import PartitionSpec as P

epsilon = 1e-06


def on_device(tokens, norm_gain, gate_train, up_train, down_train, expert_ids, route_weights):
    experts, rows, cols = gate_train.shape
    fs_at = lax.axis_index("fs")
    tok_rows, picks = expert_ids.shape
    down_rows, down_cols = down_train.shape[1:]
    fs_count = lax.axis_size("fs")
    gate_up = jnp.concatenate(
        [norm_gain[None, :, None] * gate_train, norm_gain[None, :, None] * up_train], axis=2
    ).astype(jnp.bfloat16)
    gate_up = gate_up.transpose(1, 0, 2).reshape(rows, experts * 2 * cols)
    gate_up_all = lax.all_gather(gate_up, "fs", axis=0, tiled=True)
    down_all = lax.all_gather(
        down_train.astype(jnp.bfloat16).reshape(experts * down_rows, down_cols),
        "fs",
        axis=0,
        tiled=True,
    )
    tok_float = tokens.astype(jnp.float32)
    normed = (
        tok_float * lax.rsqrt(jnp.mean(tok_float * tok_float, axis=-1, keepdims=True) + epsilon)
    ).astype(jnp.bfloat16)
    shares = route_weights / jnp.sum(route_weights, axis=-1, keepdims=True)
    group = 2 * lax.axis_size("tp")
    picked = [jnp.zeros((tok_rows, cols), jnp.float32) for _ in range(picks)]
    for first in range(0, experts, group):
        part = gate_up_all[:, first * 2 * cols : (first + group) * 2 * cols]
        if first:
            part, picked = lax.optimization_barrier((part, picked))
        acts = jnp.dot(normed, part, preferred_element_type=jnp.float32)
        for at in range(group):
            g = acts[:, at * 2 * cols : at * 2 * cols + cols]
            u = acts[:, at * 2 * cols + cols : (at + 1) * 2 * cols]
            h = jax.nn.silu(g) * u
            for k in range(picks):
                picked[k] = picked[k] + jnp.where(expert_ids[:, k : k + 1] == first + at, h, 0.0)
    hidden = jnp.stack([picked[k] * shares[:, k : k + 1] for k in range(picks)], 0)
    hidden_all = lax.all_gather(hidden.astype(jnp.bfloat16), "tp", axis=2, tiled=True)
    hidden_all = hidden_all.reshape(picks, tok_rows, fs_count, 1, down_rows)
    ids = jnp.arange(experts, dtype=jnp.int32)[None, None, :, None]
    mixed = jnp.zeros((tok_rows, down_cols), jnp.float32)
    for first in range(0, fs_count, group):
        blocks = hidden_all[:, :, first : first + group]
        if first:
            blocks, mixed = lax.optimization_barrier((blocks, mixed))
        spread = jnp.zeros((tok_rows, group, experts, down_rows), jnp.bfloat16)
        for k in range(picks):
            spread = jnp.where(expert_ids[:, k][:, None, None, None] == ids, blocks[k], spread)
        depth = experts * down_rows
        mixed = mixed + jnp.dot(
            spread.reshape(tok_rows, group * depth),
            down_all[first * depth : (first + group) * depth],
            preferred_element_type=jnp.float32,
        )
    mixed = mixed.astype(jnp.bfloat16)
    own = lax.dynamic_slice_in_dim(gate_up_all, fs_at * 2 * cols, 2 * cols, 1)
    down_own = lax.dynamic_slice_in_dim(
        down_all.reshape(fs_count, experts, down_rows, down_cols), fs_at, 1, 1
    ).reshape(1, fs_count * down_rows, down_cols)
    down_serve = lax.all_to_all(down_own, "tp", split_axis=1, concat_axis=2, tiled=True)
    return (own[None, :, :cols], own[None, :, cols:], down_serve, mixed)


def solution(mesh):
    return jax.shard_map(
        on_device,
        mesh=mesh,
        in_specs=(
            P("fs", None),
            P("fs"),
            P(None, "fs", "tp"),
            P(None, "fs", "tp"),
            P(None, "fs", "tp"),
            P("fs", None),
            P("fs", None),
        ),
        out_specs=(P("fs", None, "tp"), P("fs", None, "tp"), P("fs", "tp", None), P("fs", "tp")),
        check_vma=False,
    )
```

profile of v0, /device:TPU:0, one launch (start us, length us, event | category | flops | bytes accessed | tf_op | source)
XLA Modules:
  0.0 353.5 jit_solution(751838854216082823)
XLA Ops:
  7.2 0.0 copy-start
  7.2 0.0 all-gather.4.cloned.1.call-start
  7.2 2.3 multiply_convert_fusion.1
  9.6 0.0 copy-start.2
  9.6 0.0 copy-start.1
  9.6 1.3 pad_maximum_fusion
  10.9 0.0 all-gather.4.cloned.1.call-update
  10.9 0.0 all-gather.6.cloned.1.call-start
  10.9 0.0 copy-done
  10.9 1.0 convert_element_type.14
  11.9 0.0 all-gather.6.cloned.1.call-update
  11.9 0.0 all-gather.8.cloned.1.call-start
  12.0 0.0 copy-done.2
  12.0 0.0 copy-done.1
  12.0 0.2 compare_reduce_fusion.15
  12.2 3.1 fusion
  15.4 174.5 %all-gather.4.cloned.1.call-done = bf16[2048,3072]{0,1:T(8,128)(2,1)} async-done(((bf16[256,3072]{0,1:T(8,128)(2,1)}), bf16[2048,3072]{0,1:T(8,128)(2,1)}) %all-gather.4.cloned.1.call-update) | async-done | bytes 12582928 | tf_op jit(solution)/shard_map/all_gather | solution.py:19
  189.9 17.1 %fusion.2 = f32[1024,3072]{1,0:T(8,128)S(1)} fusion(bf16[2048,3072]{0,1:T(8,128)(2,1)} %all-gather.4.cloned.1.call-done, bf16[1024,2048]{1,0:T(8,128)(2,1)} %param.7, f32[1024]{0:T(1024)S(1)} %add_rsqrt_fusion), kind=kOutput, calls=%fused_computation.5 | convolution fusion | flops 12891193344 | bytes 29364224 | tf_op jit(solution)/shard_map/dot_general | solution.py:37
  207.0 4.5 %fusion.5 = bf16[1,1024,192]{2,1,0:T(8,128)(2,1)S(1)} fusion(f32[1024]{0:T(1024)S(1)} %bitcast.47, pred[1024]{0:T(1024)(128)(4,1)S(1)} %get-tuple-element.19, pred[1024]{0:T(1024)(128)(4,1)S(1)} %get-tuple-element.18, pred[1024]{0:T(1024)(128)(4,1)S(1)} %get-tuple-element.17, pred[1024]{0:T(1024)(128)(4,1)S(1)} %get-tuple-element.16, ...), kind=kLoop, calls=%fused_computation.24 | loop fusion | flops 11206656 | bytes 12988416 | tf_op jit(solution)/shard_map/stack | solution.py:44
  211.5 4.5 %fusion.6 = bf16[1,1024,192]{2,1,0:T(8,128)(2,1)S(1)} fusion(f32[1024]{0:T(1024)S(1)} %bitcast.46, pred[1024]{0:T(1024)(128)(4,1)S(1)} %get-tuple-element.12, pred[1024]{0:T(1024)(128)(4,1)S(1)} %get-tuple-element.11, pred[1024]{0:T(1024)(128)(4,1)S(1)} %get-tuple-element.10, pred[1024]{0:T(1024)(128)(4,1)S(1)} %get-tuple-element.9, ...), kind=kLoop, calls=%fused_computation.25 | loop fusion | flops 11206656 | bytes 12988416 | tf_op jit(solution)/shard_map/stack | solution.py:44
  216.0 0.2 pad_maximum_fusion.1
  216.2 2.0 copy.22
  218.2 0.0 all-gather.8.cloned.1.call-update
  218.2 71.3 %all-gather.6.cloned.1.call-done = bf16[6144,512]{1,0:T(8,128)(2,1)} async-done(((bf16[768,512]{1,0:T(8,128)(2,1)}), bf16[6144,512]{1,0:T(8,128)(2,1)}) %all-gather.6.cloned.1.call-update) | async-done | bytes 6291472 | tf_op jit(solution)/shard_map/all_gather | solution.py:20
  289.5 1.2 constant_dynamic-slice_fusion
  290.8 1.2 copy.30
  292.0 0.5 broadcast.126
  292.5 5.4 %reduce.32 = bf16[768,512]{1,0:T(8,128)(2,1)S(1)} reduce(bf16[768,1,512]{2,1,0:T(2,128)(2,1)S(1)} %bitcast.37, bf16[]{:T(256)} %broadcast.126), dimensions={1}, to_apply=%bitcast.32.reduce_sub_computation | reduce | bytes 1572866
  297.9 1.4 reshape.117
  299.3 3.7 %all-to-all-start = ((bf16[4,2,49152]{2,1,0:T(2,128)(2,1)}), bf16[4,2,49152]{2,1,0:T(2,128)(2,1)S(1)}, u32[]{:S(2)}, u32[]{:S(2)}) async-start(bf16[4,2,49152]{2,1,0:T(2,128)(2,1)} %reshape.117), calls=%async_computation | async-start | bytes 1572864 | tf_op jit(solution)/shard_map/all_to_all | solution.py:67
  303.0 20.2 %all-to-all-done = bf16[4,2,49152]{2,1,0:T(2,128)(2,1)S(1)} async-done(((bf16[4,2,49152]{2,1,0:T(2,128)(2,1)}), bf16[4,2,49152]{2,1,0:T(2,128)(2,1)S(1)}, u32[]{:S(2)}, u32[]{:S(2)}) %all-to-all-start) | async-done | bytes 786464 | tf_op jit(solution)/shard_map/all_to_all | solution.py:67
  323.2 0.7 reshape.118
  324.0 0.2 copy.25
  324.2 1.0 copy.28
  325.2 2.7 dynamic-slice_bitcast_fusion
  327.9 0.0 all-gather.8.cloned.1.call-done
  327.9 7.8 %fusion.7 = (bf16[1,1024,768]{1,0,2:T(2,128)(2,1)S(1)}, bf16[1,1024,768]{1,0,2:T(2,128)(2,1)S(1)}) fusion(bf16[2,1024,768]{1,0,2:T(2,128)(2,1)} %all-gather.8.cloned.1.call-done), kind=kLoop, calls=%fused_computation.47 | loop fusion | bytes 6291456 | tf_op jit(solution)/shard_map/slice | solution.py:55
  335.7 0.6 copy.26
  336.3 0.0 slice-start
  336.3 0.6 copy.27
  336.9 0.0 slice-start.1
  336.9 1.9 select_select_fusion
  338.8 0.0 slice-done
  338.8 0.5 slice-done.1
  339.3 7.6 %convolution_convert_fusion = bf16[1024,512]{1,0:T(8,128)(2,1)} fusion(bf16[1024,6144]{0,1:T(8,128)(2,1)S(1)} %bitcast.33, bf16[6144,512]{1,0:T(8,128)(2,1)S(1)} %bitcast.45), kind=kOutput, calls=%fused_computation.10 | convolution fusion | flops 6442975232 | bytes 19922944 | tf_op jit(solution)/shard_map/dot_general | solution.py:57
  (7 shorter events, 0.1 us)
Async XLA Ops:
  7.2 3.8 %copy-start = (f32[8,96,512]{2,1,0:T(8,128)S(1)}, f32[8,96,512]{2,1,0:T(8,128)}, u32[]{:S(2)}) copy-start(f32[8,96,512]{2,1,0:T(8,128)} %param.11) | copy-start | bytes 4718596
  7.2 182.7 %all-gather.4.cloned.1.call-start = ((), (), s32[]{:S(2)}) async-start(), calls=%async_computation.1 | async-start | bytes 14155776 | tf_op jit(solution)/shard_map/all_gather | solution.py:19
  9.6 2.4 copy-start.2
  9.6 2.5 copy-start.1
  10.9 278.7 %all-gather.6.cloned.1.call-start = ((), (), s32[]{:S(2)}) async-start(), calls=%async_computation.2 | async-start | bytes 7077888 | tf_op jit(solution)/shard_map/all_gather | solution.py:20
  11.9 315.9 %all-gather.8.cloned.1.call-start = ((), (), s32[]{:S(2)}) async-start(), calls=%async_computation.3 | async-start | bytes 3932160 | tf_op jit(solution)/shard_map/all_gather | solution.py:45
  299.3 23.9 %all-to-all-start = ((bf16[4,2,49152]{2,1,0:T(2,128)(2,1)}), bf16[4,2,49152]{2,1,0:T(2,128)(2,1)S(1)}, u32[]{:S(2)}, u32[]{:S(2)}) async-start(bf16[4,2,49152]{2,1,0:T(2,128)(2,1)} %reshape.117), calls=%async_computation | async-start | bytes 1572864 | tf_op jit(solution)/shard_map/all_to_all | solution.py:67
  336.3 2.5 slice-start
  336.9 2.4 slice-start.1
Sparse Core Ops, SparseCore 0:
  11.0 178.8 all-gather.3
  192.6 96.8 all-gather.5
  291.7 35.1 all-gather.7
where the time goes:
time: 354 us; the launch traced here: 353 us
  waiting for transfers between devices  266 us (75%)
  matrix products  24.7 us (7%)
  other arithmetic  24.4 us (7%)
  local copies, waits for them, and re-layouts  20.5 us (6%)
  between operations  14 us (4%)
  starting transfers between devices  3.8 us (1%)
    all_gather x1, waiting for transfers between devices, on_device(): gate_up_all = lax.all_gather(gate_up, 'fs', axis=0, tiled=True)  175 us
    all_gather x1, waiting for transfers between devices, on_device(): lax.all_gather(down_train.astype(jnp.bfloat16).reshape(experts * down_row...  71.3 us
    all_to_all x1, waiting for transfers between devices, on_device(): lax.all_to_all(down_own, 'tp', split_axis=1, concat_axis=2, tiled=True)  20.2 us
    dot_general x1, matrix products, on_device(): acts = jnp.dot(normed, part, preferred_element_type=jnp.float32)  17.1 us
    another operation x3, other arithmetic, on_device(): jnp.stack([picked[k] * shares[:, k:k + 1] for k in range(picks)], 0)  9.18 us
    slice x1, local copies, waits for them, and re-layouts, on_device(): blocks[k]  7.82 us
    dot_general x1, matrix products, on_device(): jnp.dot(spread.reshape(tok_rows, group * depth), down_all[first * depth:(...  7.64 us
  transfers between devices with their start and end apart: 4, of which 3 were waited for; matrix products, arithmetic and copies ran while one was open for 13% of the time, Pallas kernels for 0%

commit v1 on v0

--- a/solution.py
+++ b/solution.py
@@ -2,6 +2,7 @@
 import jax.numpy as jnp
 from jax import lax
 from jax.sharding import PartitionSpec as P
+from jax.lax import all_to_all, psum
 
 epsilon = 1e-06
 
@@ -64,7 +65,9 @@
     down_own = lax.dynamic_slice_in_dim(
         down_all.reshape(fs_count, experts, down_rows, down_cols), fs_at, 1, 1
     ).reshape(1, fs_count * down_rows, down_cols)
-    down_serve = lax.all_to_all(down_own, "tp", split_axis=1, concat_axis=2, tiled=True)
+    down_serve = jnp.concatenate(
+        all_to_all(jnp.stack(jnp.split(down_own, psum(1, "tp"), 1)), "tp", 0, 0), 2
+    )
     return (own[None, :, :cols], own[None, :, cols:], down_serve, mixed)
 
 

time: 354 us -> 351 us (level)
  waiting for transfers between devices: 266 us -> 272 us
  other arithmetic: 24.4 us -> 19.9 us
  local copies, waits for them, and re-layouts: 20.5 us -> 16.5 us
    all_gather x1, waiting for transfers between devices: 0.01 us -> 7.35 us  [on_device(): lax.all_gather(hidden.astype(jnp.bfloat16), 'tp', axis=2, tiled=True)]
    unnamed x2 -> x1, other arithmetic: 5.43 us -> 0.01 us
  transfers between devices with their start and end apart: 4 -> 4, of which waited for: 3 -> 4; matrix products, arithmetic and copies ran while one was open for 13% -> 11% of each run, Pallas kernels for 0% -> 0%
where the time goes in v1:
time: 351 us
  waiting for transfers between devices  272 us (77%)
  matrix products  24.7 us (7%)
  other arithmetic  19.9 us (6%)
  local copies, waits for them, and re-layouts  16.5 us (5%)
  between operations  14 us (4%)
  starting transfers between devices  3.8 us (1%)
    all_gather x1, waiting for transfers between devices, on_device(): gate_up_all = lax.all_gather(gate_up, 'fs', axis=0, tiled=True)  175 us
    all_gather x1, waiting for transfers between devices, on_device(): lax.all_gather(down_train.astype(jnp.bfloat16).reshape(experts * down_row...  71.3 us
    all_to_all x1, waiting for transfers between devices, on_device(): all_to_all(jnp.stack(jnp.split(down_own, psum(1, 'tp'), 1)), 'tp', 0, 0)  18.8 us
    dot_general x1, matrix products, on_device(): acts = jnp.dot(normed, part, preferred_element_type=jnp.float32)  17.1 us
    another operation x3, other arithmetic, on_device(): jnp.stack([picked[k] * shares[:, k:k + 1] for k in range(picks)], 0)  9.18 us
    slice x1, local copies, waits for them, and re-layouts, on_device(): blocks[k]  7.82 us
    dot_general x1, matrix products, on_device(): jnp.dot(spread.reshape(tok_rows, group * depth), down_all[first * depth:(...  7.65 us
    all_gather x1, waiting for transfers between devices, on_device(): lax.all_gather(hidden.astype(jnp.bfloat16), 'tp', axis=2, tiled=True)  7.35 us
  transfers between devices with their start and end apart: 4, of which 4 were waited for; matrix products, arithmetic and copies ran while one was open for 11% of the time, Pallas kernels for 0%

profile of v1, /device:TPU:0, one launch (start us, length us, event | category | flops | bytes accessed | tf_op | source)
XLA Modules:
  0.0 350.9 jit_solution(14751124145734465730)
XLA Ops:
  7.2 0.0 copy-start
  7.2 0.0 all-gather.4.cloned.1.call-start
  7.2 2.3 multiply_convert_fusion.1
  9.6 0.0 copy-start.2
  9.6 0.0 copy-start.1
  9.6 1.3 pad_maximum_fusion
  10.9 0.0 all-gather.4.cloned.1.call-update
  10.9 0.0 all-gather.6.cloned.1.call-start
  10.9 0.0 copy-done
  10.9 1.0 convert_element_type.14
  11.9 0.0 all-gather.6.cloned.1.call-update
  11.9 0.0 all-gather.8.cloned.1.call-start
  12.0 0.0 copy-done.2
  12.0 0.0 copy-done.1
  12.0 0.2 compare_reduce_fusion.15
  12.2 3.1 fusion
  15.4 174.5 %all-gather.4.cloned.1.call-done = bf16[2048,3072]{0,1:T(8,128)(2,1)} async-done(((bf16[256,3072]{0,1:T(8,128)(2,1)}), bf16[2048,3072]{0,1:T(8,128)(2,1)}) %all-gather.4.cloned.1.call-update) | async-done | bytes 12582928 | tf_op jit(solution)/shard_map/all_gather | solution.py:20
  189.9 17.1 %fusion.2 = f32[1024,3072]{1,0:T(8,128)S(1)} fusion(bf16[2048,3072]{0,1:T(8,128)(2,1)} %all-gather.4.cloned.1.call-done, bf16[1024,2048]{1,0:T(8,128)(2,1)} %param.7, f32[1024]{0:T(1024)S(1)} %add_rsqrt_fusion), kind=kOutput, calls=%fused_computation.5 | convolution fusion | flops 12891193344 | bytes 29364224 | tf_op jit(solution)/shard_map/dot_general | solution.py:38
  207.0 4.5 %fusion.5 = bf16[1,1024,192]{2,1,0:T(8,128)(2,1)S(1)} fusion(f32[1024]{0:T(1024)S(1)} %bitcast.47, pred[1024]{0:T(1024)(128)(4,1)S(1)} %get-tuple-element.19, pred[1024]{0:T(1024)(128)(4,1)S(1)} %get-tuple-element.18, pred[1024]{0:T(1024)(128)(4,1)S(1)} %get-tuple-element.17, pred[1024]{0:T(1024)(128)(4,1)S(1)} %get-tuple-element.16, ...), kind=kLoop, calls=%fused_computation.25 | loop fusion | flops 11206656 | bytes 12988416 | tf_op jit(solution)/shard_map/stack | solution.py:45
  211.5 4.5 %fusion.6 = bf16[1,1024,192]{2,1,0:T(8,128)(2,1)S(1)} fusion(f32[1024]{0:T(1024)S(1)} %bitcast.46, pred[1024]{0:T(1024)(128)(4,1)S(1)} %get-tuple-element.12, pred[1024]{0:T(1024)(128)(4,1)S(1)} %get-tuple-element.11, pred[1024]{0:T(1024)(128)(4,1)S(1)} %get-tuple-element.10, pred[1024]{0:T(1024)(128)(4,1)S(1)} %get-tuple-element.9, ...), kind=kLoop, calls=%fused_computation.26 | loop fusion | flops 11206656 | bytes 12988416 | tf_op jit(solution)/shard_map/stack | solution.py:45
  216.0 0.2 pad_maximum_fusion.1
  216.2 2.0 copy.21
  218.2 0.0 all-gather.8.cloned.1.call-update
  218.2 71.3 %all-gather.6.cloned.1.call-done = bf16[6144,512]{1,0:T(8,128)(2,1)} async-done(((bf16[768,512]{1,0:T(8,128)(2,1)}), bf16[6144,512]{1,0:T(8,128)(2,1)}) %all-gather.6.cloned.1.call-update) | async-done | bytes 6291472 | tf_op jit(solution)/shard_map/all_gather | solution.py:21
  289.5 1.2 constant_dynamic-slice_fusion
  290.7 0.1 slice_bitcast_fusion.3
  290.8 1.0 pad_maximum_fusion.2
  291.8 3.7 %all-to-all-start = ((bf16[4,1,192,512]{3,2,1,0:T(8,128)(2,1)}), bf16[4,1,192,512]{3,2,1,0:T(8,128)(2,1)S(1)}, u32[]{:S(2)}, u32[]{:S(2)}) async-start(bf16[4,1,192,512]{3,2,1,0:T(8,128)(2,1)} %pad_maximum_fusion.2), calls=%async_computation | async-start | bytes 1572864 | tf_op jit(solution)/shard_map/all_to_all | solution.py:69
  295.5 18.8 %all-to-all-done = bf16[4,1,192,512]{3,2,1,0:T(8,128)(2,1)S(1)} async-done(((bf16[4,1,192,512]{3,2,1,0:T(8,128)(2,1)}), bf16[4,1,192,512]{3,2,1,0:T(8,128)(2,1)S(1)}, u32[]{:S(2)}, u32[]{:S(2)}) %all-to-all-start) | async-done | bytes 786464 | tf_op jit(solution)/shard_map/all_to_all | solution.py:69
  314.3 1.0 copy.26
  315.2 2.7 dynamic-slice_bitcast_fusion
  317.9 7.4 %all-gather.8.cloned.1.call-done = bf16[2,1024,768]{1,0,2:T(2,128)(2,1)} async-done(((bf16[2,1024,192]{1,0,2:T(2,128)(2,1)}), bf16[2,1024,768]{1,0,2:T(2,128)(2,1)}) %all-gather.8.cloned.1.call-update) | async-done | bytes 3145744 | tf_op jit(solution)/shard_map/all_gather | solution.py:46
  325.3 7.8 %fusion.7 = (bf16[1,1024,768]{1,0,2:T(2,128)(2,1)S(1)}, bf16[1,1024,768]{1,0,2:T(2,128)(2,1)S(1)}) fusion(bf16[2,1024,768]{1,0,2:T(2,128)(2,1)} %all-gather.8.cloned.1.call-done), kind=kLoop, calls=%fused_computation.52 | loop fusion | bytes 6291456 | tf_op jit(solution)/shard_map/slice | solution.py:56
  333.1 0.6 copy.24
  333.7 0.0 slice-start
  333.7 0.6 copy.25
  334.3 0.0 slice-start.1
  334.3 1.9 select_select_fusion
  336.2 0.0 slice-done
  336.2 0.5 slice-done.1
  336.7 7.6 %convolution_convert_fusion = bf16[1024,512]{1,0:T(8,128)(2,1)} fusion(bf16[1024,6144]{0,1:T(8,128)(2,1)S(1)} %bitcast.35, bf16[6144,512]{1,0:T(8,128)(2,1)S(1)} %bitcast.45), kind=kOutput, calls=%fused_computation.10 | convolution fusion | flops 6442975232 | bytes 19922944 | tf_op jit(solution)/shard_map/dot_general | solution.py:58
  (7 shorter events, 0.1 us)
Async XLA Ops:
  7.2 3.8 %copy-start = (f32[8,96,512]{2,1,0:T(8,128)S(1)}, f32[8,96,512]{2,1,0:T(8,128)}, u32[]{:S(2)}) copy-start(f32[8,96,512]{2,1,0:T(8,128)} %param.11) | copy-start | bytes 4718596
  7.2 182.7 %all-gather.4.cloned.1.call-start = ((), (), s32[]{:S(2)}) async-start(), calls=%async_computation.1 | async-start | bytes 14155776 | tf_op jit(solution)/shard_map/all_gather | solution.py:20
  9.6 2.4 copy-start.2
  9.6 2.5 copy-start.1
  10.9 278.7 %all-gather.6.cloned.1.call-start = ((), (), s32[]{:S(2)}) async-start(), calls=%async_computation.2 | async-start | bytes 7077888 | tf_op jit(solution)/shard_map/all_gather | solution.py:21
  11.9 313.3 %all-gather.8.cloned.1.call-start = ((), (), s32[]{:S(2)}) async-start(), calls=%async_computation.3 | async-start | bytes 3932160 | tf_op jit(solution)/shard_map/all_gather | solution.py:46
  291.8 22.5 %all-to-all-start = ((bf16[4,1,192,512]{3,2,1,0:T(8,128)(2,1)}), bf16[4,1,192,512]{3,2,1,0:T(8,128)(2,1)S(1)}, u32[]{:S(2)}, u32[]{:S(2)}) async-start(bf16[4,1,192,512]{3,2,1,0:T(8,128)(2,1)} %pad_maximum_fusion.2), calls=%async_computation | async-start | bytes 1572864 | tf_op jit(solution)/shard_map/all_to_all | solution.py:69
  333.7 2.5 slice-start
  334.3 2.4 slice-start.1
Sparse Core Ops, SparseCore 0:
  11.0 178.8 all-gather.3
  192.6 96.8 all-gather.5
  291.7 33.5 all-gather.7
